TPU v7x, 512 devices: a whole 4x4x16 slice. The times are simulated.
512 devices in a mesh: ep: 32 (over z, core), tp: 16 (over y, x).
Axes of the slice: x: 4, y: 4, z: 16, core: 2. Of those that a mesh axis runs over, the one named last changes fastest.
Arguments:
- query_rows: bfloat16 [12288, 2048], P('ep', 'tp'), may hold values from -6 to 6
- key_rows: bfloat16 [12288, 2048], P('ep', 'tp'), may hold values from -6 to 6
- value_rows: bfloat16 [12288, 2048], P('ep', 'tp'), may hold values from -6 to 6
- second_scale: float32 [16], P('tp'), may hold values from 0.3 to 0.8
- head_gain: float32 [128], replicated, may hold values from 0.1 to 1.9
- out_weight: bfloat16 [2048, 4096], P(None, 'tp'), may hold values from -0.125 to 0.125
- routed_rows: bfloat16 [4096, 4096], P('ep', 'tp'), may hold values from -6 to 6
- norm_gain: float32 [4096], replicated, may hold values from 0.1 to 1.9
- route_ids: int32 [4096, 2], P('ep'), may hold values from 0 to 31, all different within a row; in each aligned block of 128 rows (0 to 127, 128 to 255, ...) at most 16 rows name the same one
- route_weight: float32 [4096, 2], P('ep'), may hold values from 0.1 to 0.9
- expert_gate: bfloat16 [32, 4096, 2048], P('ep', None, 'tp'), may hold values from -0.09375 to 0.09375
- expert_up: bfloat16 [32, 4096, 2048], P('ep', None, 'tp'), may hold values from -0.09375 to 0.09375
- expert_down: bfloat16 [32, 2048, 4096], P('ep', None, 'tp'), may hold values from -0.125 to 0.125
Outputs:
- mixer_out: bfloat16 [12288, 4096], P('ep', 'tp')
- expert_mix: bfloat16 [4096, 4096], P('ep', 'tp')
Inputs may be any that keep to these rules, and one draw needn't show every extreme that they name: `route_ids`: among the 128 tokens of one index of ep, no expert is named by more than 16 of them, a bound that some block reaches.
All inputs are finite; a program needn't handle non-finite values.
Results may differ from a plain program's by a relative error of at most 0.0085.
Values may be sent and summed in bfloat16 or wider, within the bound.
A program may use at most 64 MiB of HBM per device.

v0:
```python
import jax
import jax.numpy as jnp
from jax import lax
from jax.sharding import PartitionSpec as P

eps = 1e-06
head_factor = 0.8
neg_big = -1e30
key_block_rows = 1024


def side_by_side(arrays, axis, dim, along):
    both = jnp.concatenate(arrays, axis=along)
    result, at, finished = (lax.all_gather(both, axis, axis=dim, tiled=True), 0, [])
    for a in arrays:
        finished.append(lax.slice_in_dim(result, at, at + a.shape[along], axis=along))
        at += a.shape[along]
    return tuple(finished)


def rms_rows(rows_in, gain):
    floats = rows_in.astype(jnp.float32)
    factor = lax.rsqrt(jnp.mean(floats * floats, axis=-1, keepdims=True) + eps)
    return (floats * factor * gain).astype(jnp.bfloat16)


def per_device(
    query_rows,
    key_rows,
    value_rows,
    second_scale,
    head_gain,
    out_weight,
    routed_rows,
    norm_gain,
    route_ids,
    route_weight,
    expert_gate,
    expert_up,
    expert_down,
):
    count_a = query_rows.shape[0]
    per_head = second_scale.shape[0]
    head_dim = query_rows.shape[1] // (2 * per_head)
    value_dim = head_gain.shape[0]
    query_four = query_rows.reshape(count_a, per_head, 2, head_dim)
    query_pos = lax.axis_index("ep") * count_a + jnp.arange(count_a, dtype=jnp.int32)

    def key_block(carry_state, key_part, value_part, block_start):
        key_count = key_part.shape[0]
        key_four = key_part.reshape(key_count, per_head, 2, head_dim)
        value_three = value_part.reshape(key_count, per_head, value_dim)
        scores = jnp.einsum(
            "ihcd,jhcd->ihcj", query_four, key_four, preferred_element_type=jnp.float32
        ) * head_dim ** (-0.5)
        allowed = (
            query_pos[:, None] >= block_start + jnp.arange(key_count, dtype=jnp.int32)[None, :]
        )[:, None, None, :]
        scores = jnp.where(allowed, scores, neg_big)
        old_max, old_sum, old_acc = carry_state
        new_max = jnp.maximum(old_max, jnp.max(scores, axis=-1))
        weights = jnp.where(allowed, jnp.exp(scores - new_max[..., None]), 0.0)
        shrink = jnp.exp(old_max - new_max)
        new_sum = old_sum * shrink + jnp.sum(weights, axis=-1)
        update = jnp.einsum(
            "ihcj,jhe->ihce",
            weights.astype(jnp.bfloat16),
            value_three,
            preferred_element_type=jnp.float32,
        )
        return (new_max, new_sum, old_acc * shrink[..., None] + update)

    start_state = (
        jnp.full((count_a, per_head, 2), neg_big, jnp.float32),
        jnp.zeros((count_a, per_head, 2), jnp.float32),
        jnp.zeros((count_a, per_head, 2, value_dim), jnp.float32),
    )
    key_part, value_part = side_by_side((key_rows, value_rows), "ep", 0, 1)
    key_count = key_part.shape[0]

    def step_block(block_num, inner_state):
        offset_rows = block_num * key_block_rows
        key_slice = lax.dynamic_slice_in_dim(key_part, offset_rows, key_block_rows, 0)
        value_slice = lax.dynamic_slice_in_dim(value_part, offset_rows, key_block_rows, 0)
        return key_block(inner_state, key_slice, value_slice, offset_rows)

    run_max, run_sum, run_acc = lax.fori_loop(
        0, key_count // key_block_rows, step_block, start_state
    )
    maps_both = run_acc / run_sum[..., None]
    mixed_maps = maps_both[:, :, 0] - second_scale[None, :, None] * maps_both[:, :, 1]
    mean_sq = jnp.mean(mixed_maps * mixed_maps, axis=-1, keepdims=True)
    head_out = (
        (mixed_maps * lax.rsqrt(mean_sq + eps) * head_gain * head_factor)
        .astype(jnp.bfloat16)
        .reshape(count_a, per_head * value_dim)
    )
    count_b = routed_rows.shape[0]
    route_count = route_ids.shape[1]
    experts_here = expert_gate.shape[0]
    ep_devices = lax.axis_size("ep")
    expert_total = experts_here * ep_devices
    capacity = 2 * count_b * route_count // expert_total
    flat_expert = route_ids.reshape(-1)
    chosen = (flat_expert[:, None] == jnp.arange(expert_total, dtype=jnp.int32)[None, :]).astype(
        jnp.int32
    )
    ranks = jnp.sum((jnp.cumsum(chosen, axis=0) - 1) * chosen, axis=1)
    slot_of = flat_expert * capacity + ranks
    token_of = jnp.arange(count_b * route_count, dtype=jnp.int32) // route_count
    slot_token = jnp.full((expert_total * capacity,), count_b, jnp.int32).at[slot_of].set(token_of)
    padded = jnp.concatenate(
        [routed_rows, jnp.zeros((1, routed_rows.shape[1]), jnp.bfloat16)], axis=0
    )
    outgoing = padded[slot_token].reshape(ep_devices, experts_here, capacity, routed_rows.shape[1])
    column_parts = lax.all_to_all(outgoing, "ep", split_axis=0, concat_axis=0, tiled=True)
    arrived = rms_rows(lax.all_gather(column_parts, "tp", axis=3, tiled=True), norm_gain)
    gate_val = jnp.einsum(
        "sxcd,xdf->sxcf", arrived, expert_gate, preferred_element_type=jnp.float32
    )
    up_val = jnp.einsum("sxcd,xdf->sxcf", arrived, expert_up, preferred_element_type=jnp.float32)
    hidden = (jax.nn.silu(gate_val) * up_val).astype(jnp.bfloat16)
    weight_rows = out_weight
    attn_total = jnp.dot(
        lax.all_gather(
            head_out.reshape(1, 1, count_a, head_out.shape[1]), "tp", axis=3, tiled=True
        )[0, 0],
        weight_rows,
        preferred_element_type=jnp.float32,
    )
    weight_rows = expert_down
    moe_total = jnp.einsum(
        "sxcf,xfd->sxcd",
        lax.all_gather(hidden, "tp", axis=3, tiled=True),
        weight_rows,
        preferred_element_type=jnp.float32,
    )
    mixer_out = attn_total.astype(jnp.bfloat16)
    returned = lax.all_to_all(
        moe_total.astype(jnp.bfloat16), "ep", split_axis=0, concat_axis=0, tiled=True
    )
    flat_back = returned.reshape(expert_total * capacity, returned.shape[3])
    picked = flat_back[slot_of].astype(jnp.float32).reshape(count_b, route_count, returned.shape[3])
    expert_mix = jnp.sum(picked * route_weight[:, :, None], axis=1).astype(jnp.bfloat16)
    return (mixer_out, expert_mix)


def solution(mesh):
    placed = (
        P("ep", "tp"),
        P("ep", "tp"),
        P("ep", "tp"),
        P("tp"),
        P(),
        P(None, "tp"),
        P("ep", "tp"),
        P(),
        P("ep", None),
        P("ep", None),
        P("ep", None, "tp"),
        P("ep", None, "tp"),
        P("ep", None, "tp"),
    )
    return jax.shard_map(
        per_device,
        mesh=mesh,
        in_specs=placed,
        out_specs=(P("ep", "tp"), P("ep", "tp")),
        check_vma=False,
    )
```

profile of v0, /device:TPU:32, one launch (start us, length us, event | category | flops | bytes accessed | tf_op | source)
XLA Modules:
  0.0 361.6 jit_solution(12429718926275836795)
XLA Ops:
  14.6 36.4 %all_to_all.10 = bf16[32,1,16,256]{3,2,1,0:T(8,128)(2,1)} all-to-all(bf16[32,1,16,256]{3,2,1,0:T(8,128)(2,1)S(1)} %bitcast.173), channel_id=1, replica_groups=mesh['ep'=32,'tp'=16] {'ep'}, dimensions={0} | all-to-all | bytes 524288 | tf_op jit(solution)/shard_map/all_to_all | solution.py:116
  52.9 63.2 %all-gather.9.cloned.1.call-done = bf16[32,1,16,4096]{3,2,1,0:T(8,128)(2,1)} async-done(((bf16[32,1,16,256]{3,2,1,0:T(8,128)(2,1)}), bf16[32,1,16,4096]{3,2,1,0:T(8,128)(2,1)}) %all-gather.9.cloned.1.call-update) | async-done | bytes 4194320 | tf_op jit(solution)/shard_map/all_gather | solution.py:117
  116.0 3.2 fusion.24
  122.8 71.9 %all-gather.5.cloned.1.call-done = bf16[12288,256]{0,1:T(8,128)(2,1)} async-done(((bf16[384,256]{0,1:T(8,128)(2,1)}), bf16[12288,256]{0,1:T(8,128)(2,1)}) %all-gather.5.cloned.1.call-update) | async-done | bytes 6291472 | tf_op jit(solution)/shard_map/all_gather | solution.py:14
  194.7 6.2 %fusion.69 = (bf16[12288,128]{0,1:T(8,128)(2,1)}, bf16[12288,128]{0,1:T(8,128)(2,1)}) fusion(bf16[12288,256]{0,1:T(8,128)(2,1)} %all-gather.5.cloned.1.call-done), kind=kLoop, calls=%fused_computation.86 | loop fusion | bytes 12582912 | tf_op jit(solution)/shard_map/slice | solution.py:16
  200.9 94.7 %while.18 = (s32[]{:T(128)}, f32[384,1,2]{0,2,1:T(2,128)S(1)}, f32[384,1,2]{0,2,1:T(2,128)S(1)}, f32[384,1,2,128]{0,3,2,1:T(8,128)S(1)}, bf16[12288,128]{0,1:T(8...) while((s32[]{:T(128)}, f32[384,1,2]{0,2,1:T(2,128)S(1)}, ...), condition=%wide.region_3.4_spmd.clone, body=%wide.region_0.3_spmd.clone.sunk | while | flops 312907648 | bytes 25586904 | solution.py:87
  202.2 2.4 fusion.82
  204.6 3.2 fusion.85
  210.1 2.4 fusion.82
  212.5 3.2 fusion.85
  218.0 2.4 fusion.82
  220.4 3.2 fusion.85
  225.8 2.4 fusion.82
  228.3 3.2 fusion.85
  233.7 2.4 fusion.82
  236.2 3.2 fusion.85
  241.6 2.4 fusion.82
  244.1 3.2 fusion.85
  252.0 3.3 fusion.85
  259.9 3.2 fusion.85
  265.3 2.4 fusion.82
  267.8 3.2 fusion.85
  273.2 2.4 fusion.82
  275.7 3.2 fusion.85
  283.6 3.2 fusion.85
  289.0 2.4 fusion.82
  291.5 3.2 fusion.85
  296.5 3.1 fusion.48
  299.6 8.2 %all-to-all-start.1 = ((bf16[32,1,16,256]{3,2,1,0:T(8,128)(2,1)}), bf16[32,1,16,256]{3,2,1,0:T(8,128)(2,1)S(1)}, u32[]{:S(2)}, u32[]{:S(2)}) async-start(bf16[32,1,16,256]{3,2,1,0:T(8,128)(2,1)} %fusion.48), calls=%async_computation.1 | async-start | bytes 524288 | tf_op jit(solution)/shard_map/all_to_all | solution.py:139
  308.0 20.8 %all-to-all-done.1 = bf16[32,1,16,256]{3,2,1,0:T(8,128)(2,1)S(1)} async-done(((bf16[32,1,16,256]{3,2,1,0:T(8,128)(2,1)}), bf16[32,1,16,256]{3,2,1,0:T(8,128)(2,1)S(1)}, u32[]{:S(2)}, u32[]{:S(2)}) %all-to-all-start.1) | async-done | bytes 262176 | tf_op jit(solution)/shard_map/all_to_all | solution.py:139
  331.1 21.2 %all-gather.7.cloned.1.call-done = bf16[1,1,384,2048]{2,3,1,0:T(8,128)(2,1)} async-done(((bf16[1,1,384,128]{2,3,1,0:T(8,128)(2,1)}), bf16[1,1,384,2048]{2,3,1,0:T(8,128)(2,1)}) %all-gather.7.cloned.1.call-update) | async-done | bytes 1572880 | tf_op jit(solution)/shard_map/all_gather | solution.py:125
  352.4 2.7 fusion.39
  (192 shorter events, 48.4 us)
Async XLA Ops:
  7.2 289.4 %copy-start = (bf16[1,2048,256]{2,1,0:T(8,128)(2,1)S(1)}, bf16[1,2048,256]{2,1,0:T(8,128)(2,1)}, u32[]{:S(2)}) copy-start(bf16[1,2048,256]{2,1,0:T(8,128)(2,1)} %param.27) | copy-start | bytes 3145732
  7.2 43.8 %copy-start.4 = (bf16[384,128]{1,0:T(8,128)(2,1)S(1)}, bf16[384,128]{1,0:T(8,128)(2,1)}, u32[]{:S(2)}) copy-start(bf16[384,128]{1,0:T(8,128)(2,1)} %param.16) | copy-start | bytes 294916
  7.2 43.9 %copy-start.5 = (bf16[384,128]{1,0:T(8,128)(2,1)S(1)}, bf16[384,128]{1,0:T(8,128)(2,1)}, u32[]{:S(2)}) copy-start(bf16[384,128]{1,0:T(8,128)(2,1)} %param.17) | copy-start | bytes 294916
  7.2 44.9 %copy-start.6 = (bf16[384,128]{1,0:T(8,128)(2,1)S(1)}, bf16[384,128]{1,0:T(8,128)(2,1)}, u32[]{:S(2)}) copy-start(bf16[384,128]{1,0:T(8,128)(2,1)} %param.15) | copy-start | bytes 294916
  7.2 108.8 %all-gather.9.cloned.1.call-start = ((), (), s32[]{:S(2)}) async-start(), calls=%async_computation.4 | async-start | bytes 4456448 | tf_op jit(solution)/shard_map/all_gather | solution.py:117
  14.5 104.7 %copy-start.9 = (bf16[1,4096,128]{2,1,0:T(8,128)(2,1)S(1)}, bf16[1,4096,128]{2,1,0:T(8,128)(2,1)}, u32[]{:S(2)}) copy-start(bf16[1,4096,128]{2,1,0:T(8,128)(2,1)} %param.25) | copy-start | bytes 3145732
  14.5 104.7 %copy-start.11 = (f32[4096]{0:T(1024)S(1)}, f32[4096]{0:T(1024)}, u32[]{:S(2)}) copy-start(f32[4096]{0:T(1024)} %param.22) | copy-start | bytes 49156
  50.9 143.8 %all-gather.5.cloned.1.call-start = ((), (), s32[]{:S(2)}) async-start(), calls=%async_computation.2 | async-start | bytes 6488064 | tf_op jit(solution)/shard_map/all_gather | solution.py:14
  52.0 244.5 %all-gather.11.cloned.1.call-start = ((), (), s32[]{:S(2)}) async-start(), calls=%async_computation.5 | async-start | bytes 2228224 | tf_op jit(solution)/shard_map/all_gather | solution.py:134
  116.0 3.4 copy-start.2
  119.5 1.3 copy-start.10
  122.8 229.6 %all-gather.7.cloned.1.call-start = ((), (), s32[]{:S(2)}) async-start(), calls=%async_computation.3 | async-start | bytes 1671168 | tf_op jit(solution)/shard_map/all_gather | solution.py:125
  200.9 94.8 %copy-start.8 = (f32[128]{0:T(128)S(1)}, f32[128]{0:T(128)}, u32[]{:S(2)}) copy-start(f32[128]{0:T(128)} %param.19) | copy-start | bytes 1540
  204.6 3.3 copy-start.1
  212.5 3.3 copy-start.1
  220.4 3.3 copy-start.1
  228.3 3.3 copy-start.1
  236.2 3.3 copy-start.1
  244.1 3.3 copy-start.1
  252.0 3.3 copy-start.1
  259.9 3.3 copy-start.1
  267.8 3.3 copy-start.1
  275.7 3.3 copy-start.1
  283.6 3.3 copy-start.1
  291.5 3.3 copy-start.1
  295.6 12.3 %copy-start.7 = (f32[128,2]{0,1:T(2,128)S(1)}, f32[128,2]{0,1:T(2,128)}, u32[]{:S(2)}) copy-start(f32[128,2]{0,1:T(2,128)} %param.24) | copy-start | bytes 3076
  296.5 55.9 %copy-start.3 = (bf16[2048,256]{1,0:T(8,128)(2,1)S(1)}, bf16[2048,256]{1,0:T(8,128)(2,1)}, u32[]{:S(2)}) copy-start(bf16[2048,256]{1,0:T(8,128)(2,1)} %param.20) | copy-start | bytes 3145732
  299.6 29.2 %all-to-all-start.1 = ((bf16[32,1,16,256]{3,2,1,0:T(8,128)(2,1)}), bf16[32,1,16,256]{3,2,1,0:T(8,128)(2,1)S(1)}, u32[]{:S(2)}, u32[]{:S(2)}) async-start(bf16[32,1,16,256]{3,2,1,0:T(8,128)(2,1)} %fusion.48), calls=%async_computation.1 | async-start | bytes 524288 | tf_op jit(solution)/shard_map/all_to_all | solution.py:139
Sparse Core Ops, SparseCore 0:
  51.1 64.9 all-gather.8
  118.7 75.9 all-gather.4
  197.7 59.0 all-gather.10
  296.6 55.7 all-gather.6
where the time goes:
time: 362 us
  waiting for transfers between devices  177 us (49%)
  matrix products  77 us (21%)
  blocking collectives  36.4 us (10%)
  local copies, waits for them, and re-layouts  25.7 us (7%)
  other arithmetic  21.3 us (6%)
  between operations  14.7 us (4%)
  starting transfers between devices  8.4 us (2%)
    all_gather x1, waiting for transfers between devices, side_by_side(): lax.all_gather(both, axis, axis=dim, tiled=True)  71.9 us
    all_gather x1, waiting for transfers between devices, per_device(): lax.all_gather(column_parts, 'tp', axis=3, tiled=True)  63.2 us
    dot_general x12, matrix products, key_block(): jnp.einsum('ihcj,jhe->ihce', weights.astype(jnp.bfloat16), value_three, p...  38.8 us
    all_to_all x1, blocking collectives, per_device(): lax.all_to_all(outgoing, 'ep', split_axis=0, concat_axis=0, tiled=True)  36.4 us
    dot_general x12, matrix products, key_block(): jnp.einsum('ihcd,jhcd->ihcj', query_four, key_four, preferred_element_typ...  29.1 us
    all_gather x1, waiting for transfers between devices, per_device(): lax.all_gather(head_out.reshape(1, 1, count_a, head_out.shape[1]), 'tp',...  21.2 us
    all_to_all x1, waiting for transfers between devices, per_device(): lax.all_to_all(moe_total.astype(jnp.bfloat16), 'ep', split_axis=0, concat...  20.8 us
    dynamic_slice x12, local copies, waits for them, and re-layouts, step_block(): lax.dynamic_slice_in_dim(key_part, offset_rows, key_block_rows, 0)  11.7 us
  transfers between devices with their start and end apart: 5, of which 4 were waited for; matrix products, arithmetic and copies ran while one was open for 31% of the time, Pallas kernels for 0%

commit v1 on v0

--- a/solution.py
+++ b/solution.py
@@ -7,6 +7,27 @@
 head_factor = 0.8
 neg_big = -1e30
 key_block_rows = 1024
+
+
+def gather_around(x, axis, dim):
+    length, index, rows = (lax.axis_size(axis), lax.axis_index(axis), x.shape[dim])
+    upward = [(i, (i + 1) % length) for i in range(length)]
+    left = [(i, (i - 1) % length) for i in range(length)]
+    result = jnp.zeros((*x.shape[:dim], length * rows, *x.shape[dim + 1 :]), x.dtype)
+    result = lax.dynamic_update_slice_in_dim(result, x, index * rows, axis=dim)
+    from_left = from_right = x
+    halfway = length // 2
+    for hop in range(1, halfway + 1):
+        from_left = lax.ppermute(from_left, axis, upward)
+        result = lax.dynamic_update_slice_in_dim(
+            result, from_left, (index - hop) % length * rows, axis=dim
+        )
+        if hop < length - halfway:
+            from_right = lax.ppermute(from_right, axis, left)
+            result = lax.dynamic_update_slice_in_dim(
+                result, from_right, (index + hop) % length * rows, axis=dim
+            )
+    return result
 
 
 def side_by_side(arrays, axis, dim, along):
@@ -114,7 +135,7 @@
     )
     outgoing = padded[slot_token].reshape(ep_devices, experts_here, capacity, routed_rows.shape[1])
     column_parts = lax.all_to_all(outgoing, "ep", split_axis=0, concat_axis=0, tiled=True)
-    arrived = rms_rows(lax.all_gather(column_parts, "tp", axis=3, tiled=True), norm_gain)
+    arrived = rms_rows(gather_around(column_parts, "tp", 3), norm_gain)
     gate_val = jnp.einsum(
         "sxcd,xdf->sxcf", arrived, expert_gate, preferred_element_type=jnp.float32
     )

time: 362 us -> 317 us (0.88)
  waiting for transfers between devices: 177 us -> 63.1 us
  starting transfers between devices: 8.4 us -> 72.4 us
    all_gather x1, waiting for transfers between devices: 71.9 us -> 0.02 us  [side_by_side(): lax.all_gather(both, axis, axis=dim, tiled=True)]
    ppermute x0 -> x15, starting transfers between devices: none -> 66.2 us  [the longest x7 49.6 us: gather_around(): from_right = lax.ppermute(from_right, axis, left)]
    all_gather x1 -> x0, waiting for transfers between devices: 63.2 us -> none  [per_device(): lax.all_gather(column_parts, 'tp', axis=3, tiled=True)]
    ppermute x0 -> x15, waiting for transfers between devices: none -> 25.9 us  [the longest x8 25.8 us: gather_around(): from_left = lax.ppermute(from_left, axis, upward)]
    all_gather x1, waiting for transfers between devices: 21.2 us -> 16.2 us  [per_device(): lax.all_gather(head_out.reshape(1, 1, count_a, head_out.shape[1]), 'tp',...]
  transfers between devices with their start and end apart: 5 -> 19, of which waited for: 4 -> 10; matrix products, arithmetic and copies ran while one was open for 31% -> 38% of each run, Pallas kernels for 0% -> 0%
where the time goes in v1:
time: 317 us; the launch traced here: 315 us
  matrix products  76.8 us (24%)
  starting transfers between devices  72.4 us (23%)
  waiting for transfers between devices  63.1 us (20%)
  blocking collectives  39.7 us (13%)
  local copies, waits for them, and re-layouts  28.3 us (9%)
  other arithmetic  18.9 us (6%)
  between operations  15.3 us (5%)
    ppermute x7, starting transfers between devices, gather_around(): from_right = lax.ppermute(from_right, axis, left)  49.6 us
    all_to_all x1, blocking collectives, per_device(): lax.all_to_all(outgoing, 'ep', split_axis=0, concat_axis=0, tiled=True)  39.7 us
    dot_general x12, matrix products, key_block(): jnp.einsum('ihcj,jhe->ihce', weights.astype(jnp.bfloat16), value_three, p...  39 us
    dot_general x12, matrix products, key_block(): jnp.einsum('ihcd,jhcd->ihcj', query_four, key_four, preferred_element_typ...  28.8 us
    ppermute x8, waiting for transfers between devices, gather_around(): from_left = lax.ppermute(from_left, axis, upward)  25.8 us
    all_to_all x1, waiting for transfers between devices, per_device(): lax.all_to_all(moe_total.astype(jnp.bfloat16), 'ep', split_axis=0, concat...  21 us
    ppermute x8, starting transfers between devices, gather_around(): from_left = lax.ppermute(from_left, axis, upward)  16.7 us
    all_gather x1, waiting for transfers between devices, per_device(): lax.all_gather(head_out.reshape(1, 1, count_a, head_out.shape[1]), 'tp',...  16.2 us
  transfers between devices with their start and end apart: 19, of which 10 were waited for; matrix products, arithmetic and copies ran while one was open for 38% of the time, Pallas kernels for 0%

profile of v1, /device:TPU:32, one launch (start us, length us, event | category | flops | bytes accessed | tf_op | source)
XLA Modules:
  0.0 315.4 jit_solution(5394262396421483700)
XLA Ops:
  17.3 39.7 %all_to_all.10 = bf16[32,1,16,256]{3,2,1,0:T(8,128)(2,1)S(1)} all-to-all(bf16[32,1,16,256]{3,2,1,0:T(8,128)(2,1)S(1)} %bitcast.201), channel_id=1, replica_groups=mesh['ep'=32,'tp'=16] {'ep'}, dimensions={0} | all-to-all | bytes 524288 | tf_op jit(solution)/shard_map/all_to_all | solution.py:137
  57.0 3.3 %collective-permute-start = (bf16[32,1,16,256]{3,2,1,0:T(8,128)(2,1)S(1)}, bf16[32,1,16,256]{3,2,1,0:T(8,128)(2,1)S(1)}, u32[]{:S(2)}, u32[]{:S(2)}) collective-permute-start(bf16[32,1,16,256]{3,2,1,0:T(8,128)(2,1)S(1)} %all_to_all.10), channel_id=1, source_target_pairs={{0,1},{1,2},{2,3},{3,4},{4,5},{5,6},{6,7},{7,8},{8,9},{9,10},{10,1... | collective-permute-start | bytes 786440 | tf_op jit(solution)/shard_map/ppermute | solution.py:21
  60.4 5.8 %collective-permute-start.1 = (bf16[32,1,16,256]{3,2,1,0:T(8,128)(2,1)S(1)}, bf16[32,1,16,256]{3,2,1,0:T(8,128)(2,1)S(1)}, u32[]{:S(2)}, u32[]{:S(2)}) collective-permute-start(bf16[32,1,16,256]{3,2,1,0:T(8,128)(2,1)S(1)} %all_to_all.10), channel_id=1, source_target_pairs={{0,15},{1,0},{2,1},{3,2},{4,3},{5,4},{6,5},{7,6},{8,7},{9,8},{10,9... | collective-permute-start | bytes 786440 | tf_op jit(solution)/shard_map/ppermute | solution.py:26
  71.0 7.2 %collective-permute-start.3 = (bf16[32,1,16,256]{3,2,1,0:T(8,128)(2,1)S(1)}, bf16[32,1,16,256]{3,2,1,0:T(8,128)(2,1)S(1)}, u32[]{:S(2)}, u32[]{:S(2)}) collective-permute-start(bf16[32,1,16,256]{3,2,1,0:T(8,128)(2,1)S(1)} %collective-permute-done.1), channel_id=1, source_target_pairs={{0,15},{1,0},{2,1},{3,2},{4,3},{5,4},{6,5},{7,6},{8,7},{9,8},{10,9... | collective-permute-start | bytes 786440 | tf_op jit(solution)/shard_map/ppermute | solution.py:26
  82.6 7.2 %collective-permute-start.5 = (bf16[32,1,16,256]{3,2,1,0:T(8,128)(2,1)S(1)}, bf16[32,1,16,256]{3,2,1,0:T(8,128)(2,1)S(1)}, u32[]{:S(2)}, u32[]{:S(2)}) collective-permute-start(bf16[32,1,16,256]{3,2,1,0:T(8,128)(2,1)S(1)} %collective-permute-done.3), channel_id=1, source_target_pairs={{0,15},{1,0},{2,1},{3,2},{4,3},{5,4},{6,5},{7,6},{8,7},{9,8},{10,9... | collective-permute-start | bytes 786440 | tf_op jit(solution)/shard_map/ppermute | solution.py:26
  94.2 7.2 %collective-permute-start.7 = (bf16[32,1,16,256]{3,2,1,0:T(8,128)(2,1)S(1)}, bf16[32,1,16,256]{3,2,1,0:T(8,128)(2,1)S(1)}, u32[]{:S(2)}, u32[]{:S(2)}) collective-permute-start(bf16[32,1,16,256]{3,2,1,0:T(8,128)(2,1)S(1)} %collective-permute-done.5), channel_id=1, source_target_pairs={{0,15},{1,0},{2,1},{3,2},{4,3},{5,4},{6,5},{7,6},{8,7},{9,8},{10,9... | collective-permute-start | bytes 786440 | tf_op jit(solution)/shard_map/ppermute | solution.py:26
  105.8 7.2 %collective-permute-start.9 = (bf16[32,1,16,256]{3,2,1,0:T(8,128)(2,1)S(1)}, bf16[32,1,16,256]{3,2,1,0:T(8,128)(2,1)S(1)}, u32[]{:S(2)}, u32[]{:S(2)}) collective-permute-start(bf16[32,1,16,256]{3,2,1,0:T(8,128)(2,1)S(1)} %collective-permute-done.7), channel_id=1, source_target_pairs={{0,15},{1,0},{2,1},{3,2},{4,3},{5,4},{6,5},{7,6},{8,7},{9,8},{10,9... | collective-permute-start | bytes 786440 | tf_op jit(solution)/shard_map/ppermute | solution.py:26
  117.3 7.2 %collective-permute-start.11 = (bf16[32,1,16,256]{3,2,1,0:T(8,128)(2,1)S(1)}, bf16[32,1,16,256]{3,2,1,0:T(8,128)(2,1)S(1)}, u32[]{:S(2)}, u32[]{:S(2)}) collective-permute-start(bf16[32,1,16,256]{3,2,1,0:T(8,128)(2,1)S(1)} %collective-permute-done.9), channel_id=1, source_target_pairs={{0,15},{1,0},{2,1},{3,2},{4,3},{5,4},{6,5},{7,6},{8,7},{9,8},{10,9... | collective-permute-start | bytes 786440 | tf_op jit(solution)/shard_map/ppermute | solution.py:26
  124.7 2.5 collective-permute-done.10
  129.1 7.5 %collective-permute-start.13 = (bf16[32,1,16,256]{3,2,1,0:T(8,128)(2,1)S(1)}, bf16[32,1,16,256]{3,2,1,0:T(8,128)(2,1)S(1)}, u32[]{:S(2)}, u32[]{:S(2)}) collective-permute-start(bf16[32,1,16,256]{3,2,1,0:T(8,128)(2,1)S(1)} %collective-permute-done.11), channel_id=1, source_target_pairs={{0,15},{1,0},{2,1},{3,2},{4,3},{5,4},{6,5},{7,6},{8,7},{9,8},{10,9... | collective-permute-start | bytes 786440 | tf_op jit(solution)/shard_map/ppermute | solution.py:26
  136.7 3.3 %collective-permute-done.12 = bf16[32,1,16,256]{3,2,1,0:T(8,128)(2,1)S(1)} collective-permute-done((bf16[32,1,16,256]{3,2,1,0:T(8,128)(2,1)S(1)}, bf16[32,1,16,256]{3,2,1,0:T(8,128)(2,1)S(1)}, u32[]{:S(2)}, u32[]{:S(2)}) %collective-permute-start.12) | collective-permute-done | bytes 262176 | tf_op jit(solution)/shard_map/ppermute | solution.py:21
  142.0 9.6 %collective-permute-done.14 = bf16[32,1,16,256]{3,2,1,0:T(8,128)(2,1)S(1)} collective-permute-done((bf16[32,1,16,256]{3,2,1,0:T(8,128)(2,1)S(1)}, bf16[32,1,16,256]{3,2,1,0:T(8,128)(2,1)S(1)}, u32[]{:S(2)}, u32[]{:S(2)}) %collective-permute-start.14) | collective-permute-done | bytes 262176 | tf_op jit(solution)/shard_map/ppermute | solution.py:21
  156.1 6.2 %fusion.63 = (bf16[12288,128]{0,1:T(8,128)(2,1)}, bf16[12288,128]{0,1:T(8,128)(2,1)}) fusion(bf16[12288,256]{0,1:T(8,128)(2,1)} %all-gather.4.cloned.1.call-done), kind=kLoop, calls=%fused_computation.101 | loop fusion | bytes 12582912 | tf_op jit(solution)/shard_map/slice | solution.py:37
  162.3 94.5 %while.18 = (s32[]{:T(128)}, f32[384,1,2]{0,2,1:T(2,128)S(1)}, f32[384,1,2]{0,2,1:T(2,128)S(1)}, f32[384,1,2,128]{0,3,2,1:T(8,128)S(1)}, bf16[12288,128]{0,1:T(8...) while((s32[]{:T(128)}, f32[384,1,2]{0,2,1:T(2,128)S(1)}, ...), condition=%wide.region_3.4_spmd.clone, body=%wide.region_0.3_spmd.clone.sunk | while | flops 312907648 | bytes 25586904 | solution.py:108
  163.6 2.4 fusion.76
  166.0 3.2 %fusion.79 = f32[384,1,2,128]{0,3,2,1:T(8,128)S(1)} fusion(f32[2,1024,384]{2,1,0:T(8,128)} %get-tuple-element.251, f32[384,2]{0,1:T(2,128)S(1)} %bitcast.199, pred[384,1024]{0,1:T(8,128)(4,1)S(1)} %broadcast_compare_fusion.2, f32[384,1,2,128]{0,3,2,1:T(8,128)S(1)} %get-tuple-element.268, bf16[12288,128]{0,1:T(8,128)(2,1)} %get-tuple-element.283, ...), kind=kOutput, calls=%fused_computation.13.clone.1 | convolution fusion | flops 205553664 | bytes 4593669 | tf_op jit(solution)/shard_map/while/body/eval_jaxpr/ihcj,jhe->ihce/dot_general | solution.py:86
  173.9 3.2 %fusion.79 = f32[384,1,2,128]{0,3,2,1:T(8,128)S(1)} fusion(f32[2,1024,384]{2,1,0:T(8,128)} %get-tuple-element.251, f32[384,2]{0,1:T(2,128)S(1)} %bitcast.199, pred[384,1024]{0,1:T(8,128)(4,1)S(1)} %broadcast_compare_fusion.2, f32[384,1,2,128]{0,3,2,1:T(8,128)S(1)} %get-tuple-element.268, bf16[12288,128]{0,1:T(8,128)(2,1)} %get-tuple-element.283, ...), kind=kOutput, calls=%fused_computation.13.clone.1 | convolution fusion | flops 205553664 | bytes 4593669 | tf_op jit(solution)/shard_map/while/body/eval_jaxpr/ihcj,jhe->ihce/dot_general | solution.py:86
  181.7 3.2 %fusion.79 = f32[384,1,2,128]{0,3,2,1:T(8,128)S(1)} fusion(f32[2,1024,384]{2,1,0:T(8,128)} %get-tuple-element.251, f32[384,2]{0,1:T(2,128)S(1)} %bitcast.199, pred[384,1024]{0,1:T(8,128)(4,1)S(1)} %broadcast_compare_fusion.2, f32[384,1,2,128]{0,3,2,1:T(8,128)S(1)} %get-tuple-element.268, bf16[12288,128]{0,1:T(8,128)(2,1)} %get-tuple-element.283, ...), kind=kOutput, calls=%fused_computation.13.clone.1 | convolution fusion | flops 205553664 | bytes 4593669 | tf_op jit(solution)/shard_map/while/body/eval_jaxpr/ihcj,jhe->ihce/dot_general | solution.py:86
  189.6 3.3 %fusion.79 = f32[384,1,2,128]{0,3,2,1:T(8,128)S(1)} fusion(f32[2,1024,384]{2,1,0:T(8,128)} %get-tuple-element.251, f32[384,2]{0,1:T(2,128)S(1)} %bitcast.199, pred[384,1024]{0,1:T(8,128)(4,1)S(1)} %broadcast_compare_fusion.2, f32[384,1,2,128]{0,3,2,1:T(8,128)S(1)} %get-tuple-element.268, bf16[12288,128]{0,1:T(8,128)(2,1)} %get-tuple-element.283, ...), kind=kOutput, calls=%fused_computation.13.clone.1 | convolution fusion | flops 205553664 | bytes 4593669 | tf_op jit(solution)/shard_map/while/body/eval_jaxpr/ihcj,jhe->ihce/dot_general | solution.py:86
  197.5 3.4 %fusion.79 = f32[384,1,2,128]{0,3,2,1:T(8,128)S(1)} fusion(f32[2,1024,384]{2,1,0:T(8,128)} %get-tuple-element.251, f32[384,2]{0,1:T(2,128)S(1)} %bitcast.199, pred[384,1024]{0,1:T(8,128)(4,1)S(1)} %broadcast_compare_fusion.2, f32[384,1,2,128]{0,3,2,1:T(8,128)S(1)} %get-tuple-element.268, bf16[12288,128]{0,1:T(8,128)(2,1)} %get-tuple-element.283, ...), kind=kOutput, calls=%fused_computation.13.clone.1 | convolution fusion | flops 205553664 | bytes 4593669 | tf_op jit(solution)/shard_map/while/body/eval_jaxpr/ihcj,jhe->ihce/dot_general | solution.py:86
  205.5 3.2 %fusion.79 = f32[384,1,2,128]{0,3,2,1:T(8,128)S(1)} fusion(f32[2,1024,384]{2,1,0:T(8,128)} %get-tuple-element.251, f32[384,2]{0,1:T(2,128)S(1)} %bitcast.199, pred[384,1024]{0,1:T(8,128)(4,1)S(1)} %broadcast_compare_fusion.2, f32[384,1,2,128]{0,3,2,1:T(8,128)S(1)} %get-tuple-element.268, bf16[12288,128]{0,1:T(8,128)(2,1)} %get-tuple-element.283, ...), kind=kOutput, calls=%fused_computation.13.clone.1 | convolution fusion | flops 205553664 | bytes 4593669 | tf_op jit(solution)/shard_map/while/body/eval_jaxpr/ihcj,jhe->ihce/dot_general | solution.py:86
  213.3 3.2 %fusion.79 = f32[384,1,2,128]{0,3,2,1:T(8,128)S(1)} fusion(f32[2,1024,384]{2,1,0:T(8,128)} %get-tuple-element.251, f32[384,2]{0,1:T(2,128)S(1)} %bitcast.199, pred[384,1024]{0,1:T(8,128)(4,1)S(1)} %broadcast_compare_fusion.2, f32[384,1,2,128]{0,3,2,1:T(8,128)S(1)} %get-tuple-element.268, bf16[12288,128]{0,1:T(8,128)(2,1)} %get-tuple-element.283, ...), kind=kOutput, calls=%fused_computation.13.clone.1 | convolution fusion | flops 205553664 | bytes 4593669 | tf_op jit(solution)/shard_map/while/body/eval_jaxpr/ihcj,jhe->ihce/dot_general | solution.py:86
  221.2 3.2 %fusion.79 = f32[384,1,2,128]{0,3,2,1:T(8,128)S(1)} fusion(f32[2,1024,384]{2,1,0:T(8,128)} %get-tuple-element.251, f32[384,2]{0,1:T(2,128)S(1)} %bitcast.199, pred[384,1024]{0,1:T(8,128)(4,1)S(1)} %broadcast_compare_fusion.2, f32[384,1,2,128]{0,3,2,1:T(8,128)S(1)} %get-tuple-element.268, bf16[12288,128]{0,1:T(8,128)(2,1)} %get-tuple-element.283, ...), kind=kOutput, calls=%fused_computation.13.clone.1 | convolution fusion | flops 205553664 | bytes 4593669 | tf_op jit(solution)/shard_map/while/body/eval_jaxpr/ihcj,jhe->ihce/dot_general | solution.py:86
  229.1 3.2 %fusion.79 = f32[384,1,2,128]{0,3,2,1:T(8,128)S(1)} fusion(f32[2,1024,384]{2,1,0:T(8,128)} %get-tuple-element.251, f32[384,2]{0,1:T(2,128)S(1)} %bitcast.199, pred[384,1024]{0,1:T(8,128)(4,1)S(1)} %broadcast_compare_fusion.2, f32[384,1,2,128]{0,3,2,1:T(8,128)S(1)} %get-tuple-element.268, bf16[12288,128]{0,1:T(8,128)(2,1)} %get-tuple-element.283, ...), kind=kOutput, calls=%fused_computation.13.clone.1 | convolution fusion | flops 205553664 | bytes 4593669 | tf_op jit(solution)/shard_map/while/body/eval_jaxpr/ihcj,jhe->ihce/dot_general | solution.py:86
  236.9 3.2 %fusion.79 = f32[384,1,2,128]{0,3,2,1:T(8,128)S(1)} fusion(f32[2,1024,384]{2,1,0:T(8,128)} %get-tuple-element.251, f32[384,2]{0,1:T(2,128)S(1)} %bitcast.199, pred[384,1024]{0,1:T(8,128)(4,1)S(1)} %broadcast_compare_fusion.2, f32[384,1,2,128]{0,3,2,1:T(8,128)S(1)} %get-tuple-element.268, bf16[12288,128]{0,1:T(8,128)(2,1)} %get-tuple-element.283, ...), kind=kOutput, calls=%fused_computation.13.clone.1 | convolution fusion | flops 205553664 | bytes 4593669 | tf_op jit(solution)/shard_map/while/body/eval_jaxpr/ihcj,jhe->ihce/dot_general | solution.py:86
  244.8 3.2 %fusion.79 = f32[384,1,2,128]{0,3,2,1:T(8,128)S(1)} fusion(f32[2,1024,384]{2,1,0:T(8,128)} %get-tuple-element.251, f32[384,2]{0,1:T(2,128)S(1)} %bitcast.199, pred[384,1024]{0,1:T(8,128)(4,1)S(1)} %broadcast_compare_fusion.2, f32[384,1,2,128]{0,3,2,1:T(8,128)S(1)} %get-tuple-element.268, bf16[12288,128]{0,1:T(8,128)(2,1)} %get-tuple-element.283, ...), kind=kOutput, calls=%fused_computation.13.clone.1 | convolution fusion | flops 205553664 | bytes 4593669 | tf_op jit(solution)/shard_map/while/body/eval_jaxpr/ihcj,jhe->ihce/dot_general | solution.py:86
  252.6 3.2 %fusion.79 = f32[384,1,2,128]{0,3,2,1:T(8,128)S(1)} fusion(f32[2,1024,384]{2,1,0:T(8,128)} %get-tuple-element.251, f32[384,2]{0,1:T(2,128)S(1)} %bitcast.199, pred[384,1024]{0,1:T(8,128)(4,1)S(1)} %broadcast_compare_fusion.2, f32[384,1,2,128]{0,3,2,1:T(8,128)S(1)} %get-tuple-element.268, bf16[12288,128]{0,1:T(8,128)(2,1)} %get-tuple-element.283, ...), kind=kOutput, calls=%fused_computation.13.clone.1 | convolution fusion | flops 205553664 | bytes 4593669 | tf_op jit(solution)/shard_map/while/body/eval_jaxpr/ihcj,jhe->ihce/dot_general | solution.py:86
  257.7 3.0 fusion.48
  260.7 5.9 %all-to-all-start.1 = ((bf16[32,1,16,256]{3,2,1,0:T(8,128)(2,1)}), bf16[32,1,16,256]{3,2,1,0:T(8,128)(2,1)S(1)}, u32[]{:S(2)}, u32[]{:S(2)}) async-start(bf16[32,1,16,256]{3,2,1,0:T(8,128)(2,1)} %fusion.48), calls=%async_computation.1 | async-start | bytes 524288 | tf_op jit(solution)/shard_map/all_to_all | solution.py:160
  266.7 21.0 %all-to-all-done.1 = bf16[32,1,16,256]{3,2,1,0:T(8,128)(2,1)S(1)} async-done(((bf16[32,1,16,256]{3,2,1,0:T(8,128)(2,1)}), bf16[32,1,16,256]{3,2,1,0:T(8,128)(2,1)S(1)}, u32[]{:S(2)}, u32[]{:S(2)}) %all-to-all-start.1) | async-done | bytes 262176 | tf_op jit(solution)/shard_map/all_to_all | solution.py:160
  290.0 16.2 %all-gather.6.cloned.1.call-done = bf16[1,1,384,2048]{2,3,1,0:T(8,128)(2,1)} async-done(((bf16[1,1,384,128]{2,3,1,0:T(8,128)(2,1)}), bf16[1,1,384,2048]{2,3,1,0:T(8,128)(2,1)}) %all-gather.6.cloned.1.call-update) | async-done | bytes 1572880 | tf_op jit(solution)/shard_map/all_gather | solution.py:146
  306.2 2.7 fusion.39
  (230 shorter events, 94.9 us)
Async XLA Ops:
  7.2 250.5 %copy-start = (bf16[1,2048,256]{2,1,0:T(8,128)(2,1)S(1)}, bf16[1,2048,256]{2,1,0:T(8,128)(2,1)}, u32[]{:S(2)}) copy-start(bf16[1,2048,256]{2,1,0:T(8,128)(2,1)} %param.27) | copy-start | bytes 3145732
  7.2 59.3 %copy-start.3 = (bf16[384,128]{1,0:T(8,128)(2,1)S(1)}, bf16[384,128]{1,0:T(8,128)(2,1)}, u32[]{:S(2)}) copy-start(bf16[384,128]{1,0:T(8,128)(2,1)} %param.15) | copy-start | bytes 294916
  7.2 148.9 %all-gather.4.cloned.1.call-start = ((), (), s32[]{:S(2)}) async-start(), calls=%async_computation.2 | async-start | bytes 6488064 | tf_op jit(solution)/shard_map/all_gather | solution.py:35
  10.1 247.6 %all-gather.8.cloned.1.call-start = ((), (), s32[]{:S(2)}) async-start(), calls=%async_computation.4 | async-start | bytes 2228224 | tf_op jit(solution)/shard_map/all_gather | solution.py:155
  57.0 12.1 %collective-permute-start = (bf16[32,1,16,256]{3,2,1,0:T(8,128)(2,1)S(1)}, bf16[32,1,16,256]{3,2,1,0:T(8,128)(2,1)S(1)}, u32[]{:S(2)}, u32[]{:S(2)}) collective-permute-start(bf16[32,1,16,256]{3,2,1,0:T(8,128)(2,1)S(1)} %all_to_all.10), channel_id=1, source_target_pairs={{0,1},{1,2},{2,3},{3,4},{4,5},{5,6},{6,7},{7,8},{8,9},{9,10},{10,1... | collective-permute-start | bytes 786440 | tf_op jit(solution)/shard_map/ppermute | solution.py:21
  60.4 10.7 %collective-permute-start.1 = (bf16[32,1,16,256]{3,2,1,0:T(8,128)(2,1)S(1)}, bf16[32,1,16,256]{3,2,1,0:T(8,128)(2,1)S(1)}, u32[]{:S(2)}, u32[]{:S(2)}) collective-permute-start(bf16[32,1,16,256]{3,2,1,0:T(8,128)(2,1)S(1)} %all_to_all.10), channel_id=1, source_target_pairs={{0,15},{1,0},{2,1},{3,2},{4,3},{5,4},{6,5},{7,6},{8,7},{9,8},{10,9... | collective-permute-start | bytes 786440 | tf_op jit(solution)/shard_map/ppermute | solution.py:26
  69.1 11.6 %collective-permute-start.2 = (bf16[32,1,16,256]{3,2,1,0:T(8,128)(2,1)S(1)}, bf16[32,1,16,256]{3,2,1,0:T(8,128)(2,1)S(1)}, u32[]{:S(2)}, u32[]{:S(2)}) collective-permute-start(bf16[32,1,16,256]{3,2,1,0:T(8,128)(2,1)S(1)} %collective-permute-done), channel_id=1, source_target_pairs={{0,1},{1,2},{2,3},{3,4},{4,5},{5,6},{6,7},{7,8},{8,9},{9,10},{10,1... | collective-permute-start | bytes 786440 | tf_op jit(solution)/shard_map/ppermute | solution.py:21
  71.0 11.6 %collective-permute-start.3 = (bf16[32,1,16,256]{3,2,1,0:T(8,128)(2,1)S(1)}, bf16[32,1,16,256]{3,2,1,0:T(8,128)(2,1)S(1)}, u32[]{:S(2)}, u32[]{:S(2)}) collective-permute-start(bf16[32,1,16,256]{3,2,1,0:T(8,128)(2,1)S(1)} %collective-permute-done.1), channel_id=1, source_target_pairs={{0,15},{1,0},{2,1},{3,2},{4,3},{5,4},{6,5},{7,6},{8,7},{9,8},{10,9... | collective-permute-start | bytes 786440 | tf_op jit(solution)/shard_map/ppermute | solution.py:26
  80.7 11.6 %collective-permute-start.4 = (bf16[32,1,16,256]{3,2,1,0:T(8,128)(2,1)S(1)}, bf16[32,1,16,256]{3,2,1,0:T(8,128)(2,1)S(1)}, u32[]{:S(2)}, u32[]{:S(2)}) collective-permute-start(bf16[32,1,16,256]{3,2,1,0:T(8,128)(2,1)S(1)} %collective-permute-done.2), channel_id=1, source_target_pairs={{0,1},{1,2},{2,3},{3,4},{4,5},{5,6},{6,7},{7,8},{8,9},{9,10},{10,1... | collective-permute-start | bytes 786440 | tf_op jit(solution)/shard_map/ppermute | solution.py:21
  82.6 11.6 %collective-permute-start.5 = (bf16[32,1,16,256]{3,2,1,0:T(8,128)(2,1)S(1)}, bf16[32,1,16,256]{3,2,1,0:T(8,128)(2,1)S(1)}, u32[]{:S(2)}, u32[]{:S(2)}) collective-permute-start(bf16[32,1,16,256]{3,2,1,0:T(8,128)(2,1)S(1)} %collective-permute-done.3), channel_id=1, source_target_pairs={{0,15},{1,0},{2,1},{3,2},{4,3},{5,4},{6,5},{7,6},{8,7},{9,8},{10,9... | collective-permute-start | bytes 786440 | tf_op jit(solution)/shard_map/ppermute | solution.py:26
  92.3 11.6 %collective-permute-start.6 = (bf16[32,1,16,256]{3,2,1,0:T(8,128)(2,1)S(1)}, bf16[32,1,16,256]{3,2,1,0:T(8,128)(2,1)S(1)}, u32[]{:S(2)}, u32[]{:S(2)}) collective-permute-start(bf16[32,1,16,256]{3,2,1,0:T(8,128)(2,1)S(1)} %collective-permute-done.4), channel_id=1, source_target_pairs={{0,1},{1,2},{2,3},{3,4},{4,5},{5,6},{6,7},{7,8},{8,9},{9,10},{10,1... | collective-permute-start | bytes 786440 | tf_op jit(solution)/shard_map/ppermute | solution.py:21
  94.2 11.6 %collective-permute-start.7 = (bf16[32,1,16,256]{3,2,1,0:T(8,128)(2,1)S(1)}, bf16[32,1,16,256]{3,2,1,0:T(8,128)(2,1)S(1)}, u32[]{:S(2)}, u32[]{:S(2)}) collective-permute-start(bf16[32,1,16,256]{3,2,1,0:T(8,128)(2,1)S(1)} %collective-permute-done.5), channel_id=1, source_target_pairs={{0,15},{1,0},{2,1},{3,2},{4,3},{5,4},{6,5},{7,6},{8,7},{9,8},{10,9... | collective-permute-start | bytes 786440 | tf_op jit(solution)/shard_map/ppermute | solution.py:26
  103.8 11.6 %collective-permute-start.8 = (bf16[32,1,16,256]{3,2,1,0:T(8,128)(2,1)S(1)}, bf16[32,1,16,256]{3,2,1,0:T(8,128)(2,1)S(1)}, u32[]{:S(2)}, u32[]{:S(2)}) collective-permute-start(bf16[32,1,16,256]{3,2,1,0:T(8,128)(2,1)S(1)} %collective-permute-done.6), channel_id=1, source_target_pairs={{0,1},{1,2},{2,3},{3,4},{4,5},{5,6},{6,7},{7,8},{8,9},{9,10},{10,1... | collective-permute-start | bytes 786440 | tf_op jit(solution)/shard_map/ppermute | solution.py:21
  105.8 11.6 %collective-permute-start.9 = (bf16[32,1,16,256]{3,2,1,0:T(8,128)(2,1)S(1)}, bf16[32,1,16,256]{3,2,1,0:T(8,128)(2,1)S(1)}, u32[]{:S(2)}, u32[]{:S(2)}) collective-permute-start(bf16[32,1,16,256]{3,2,1,0:T(8,128)(2,1)S(1)} %collective-permute-done.7), channel_id=1, source_target_pairs={{0,15},{1,0},{2,1},{3,2},{4,3},{5,4},{6,5},{7,6},{8,7},{9,8},{10,9... | collective-permute-start | bytes 786440 | tf_op jit(solution)/shard_map/ppermute | solution.py:26
  113.0 39.5 %copy-start.6 = (bf16[1,4096,128]{2,1,0:T(8,128)(2,1)S(1)}, bf16[1,4096,128]{2,1,0:T(8,128)(2,1)}, u32[]{:S(2)}) copy-start(bf16[1,4096,128]{2,1,0:T(8,128)(2,1)} %param.25) | copy-start | bytes 3145732
  113.1 39.5 %copy-start.8 = (f32[4096]{0:T(1024)S(1)}, f32[4096]{0:T(1024)}, u32[]{:S(2)}) copy-start(f32[4096]{0:T(1024)} %param.22) | copy-start | bytes 49156
  115.4 11.7 %collective-permute-start.10 = (bf16[32,1,16,256]{3,2,1,0:T(8,128)(2,1)S(1)}, bf16[32,1,16,256]{3,2,1,0:T(8,128)(2,1)S(1)}, u32[]{:S(2)}, u32[]{:S(2)}) collective-permute-start(bf16[32,1,16,256]{3,2,1,0:T(8,128)(2,1)S(1)} %collective-permute-done.8), channel_id=1, source_target_pairs={{0,1},{1,2},{2,3},{3,4},{4,5},{5,6},{6,7},{7,8},{8,9},{9,10},{10,1... | collective-permute-start | bytes 786440 | tf_op jit(solution)/shard_map/ppermute | solution.py:21
  117.3 11.7 %collective-permute-start.11 = (bf16[32,1,16,256]{3,2,1,0:T(8,128)(2,1)S(1)}, bf16[32,1,16,256]{3,2,1,0:T(8,128)(2,1)S(1)}, u32[]{:S(2)}, u32[]{:S(2)}) collective-permute-start(bf16[32,1,16,256]{3,2,1,0:T(8,128)(2,1)S(1)} %collective-permute-done.9), channel_id=1, source_target_pairs={{0,15},{1,0},{2,1},{3,2},{4,3},{5,4},{6,5},{7,6},{8,7},{9,8},{10,9... | collective-permute-start | bytes 786440 | tf_op jit(solution)/shard_map/ppermute | solution.py:26
  127.1 12.9 %collective-permute-start.12 = (bf16[32,1,16,256]{3,2,1,0:T(8,128)(2,1)S(1)}, bf16[32,1,16,256]{3,2,1,0:T(8,128)(2,1)S(1)}, u32[]{:S(2)}, u32[]{:S(2)}) collective-permute-start(bf16[32,1,16,256]{3,2,1,0:T(8,128)(2,1)S(1)} %collective-permute-done.10), channel_id=1, source_target_pairs={{0,1},{1,2},{2,3},{3,4},{4,5},{5,6},{6,7},{7,8},{8,9},{9,10},{10,1... | collective-permute-start | bytes 786440 | tf_op jit(solution)/shard_map/ppermute | solution.py:21
  129.1 12.9 %collective-permute-start.13 = (bf16[32,1,16,256]{3,2,1,0:T(8,128)(2,1)S(1)}, bf16[32,1,16,256]{3,2,1,0:T(8,128)(2,1)S(1)}, u32[]{:S(2)}, u32[]{:S(2)}) collective-permute-start(bf16[32,1,16,256]{3,2,1,0:T(8,128)(2,1)S(1)} %collective-permute-done.11), channel_id=1, source_target_pairs={{0,15},{1,0},{2,1},{3,2},{4,3},{5,4},{6,5},{7,6},{8,7},{9,8},{10,9... | collective-permute-start | bytes 786440 | tf_op jit(solution)/shard_map/ppermute | solution.py:26
  140.0 11.6 %collective-permute-start.14 = (bf16[32,1,16,256]{3,2,1,0:T(8,128)(2,1)S(1)}, bf16[32,1,16,256]{3,2,1,0:T(8,128)(2,1)S(1)}, u32[]{:S(2)}, u32[]{:S(2)}) collective-permute-start(bf16[32,1,16,256]{3,2,1,0:T(8,128)(2,1)S(1)} %collective-permute-done.12), channel_id=1, source_target_pairs={{0,1},{1,2},{2,3},{3,4},{4,5},{5,6},{6,7},{7,8},{8,9},{9,10},{10,1... | collective-permute-start | bytes 786440 | tf_op jit(solution)/shard_map/ppermute | solution.py:21
  155.9 150.3 %all-gather.6.cloned.1.call-start = ((), (), s32[]{:S(2)}) async-start(), calls=%async_computation.3 | async-start | bytes 1671168 | tf_op jit(solution)/shard_map/all_gather | solution.py:146
  162.3 94.6 %copy-start.5 = (f32[128]{0:T(128)S(1)}, f32[128]{0:T(128)}, u32[]{:S(2)}) copy-start(f32[128]{0:T(128)} %param.19) | copy-start | bytes 1540
  189.6 3.3 %copy-start.1 = (f32[2,1024,384]{2,1,0:T(8,128)S(1)}, f32[2,1024,384]{2,1,0:T(8,128)}, u32[]{:S(2)}) copy-start(f32[2,1024,384]{2,1,0:T(8,128)} %get-tuple-element.251) | copy-start | bytes 9437188 | tf_op jit(solution)/shard_map/while
  197.5 3.4 %copy-start.1 = (f32[2,1024,384]{2,1,0:T(8,128)S(1)}, f32[2,1024,384]{2,1,0:T(8,128)}, u32[]{:S(2)}) copy-start(f32[2,1024,384]{2,1,0:T(8,128)} %get-tuple-element.251) | copy-start | bytes 9437188 | tf_op jit(solution)/shard_map/while
  205.5 3.3 %copy-start.1 = (f32[2,1024,384]{2,1,0:T(8,128)S(1)}, f32[2,1024,384]{2,1,0:T(8,128)}, u32[]{:S(2)}) copy-start(f32[2,1024,384]{2,1,0:T(8,128)} %get-tuple-element.251) | copy-start | bytes 9437188 | tf_op jit(solution)/shard_map/while
  213.3 3.3 %copy-start.1 = (f32[2,1024,384]{2,1,0:T(8,128)S(1)}, f32[2,1024,384]{2,1,0:T(8,128)}, u32[]{:S(2)}) copy-start(f32[2,1024,384]{2,1,0:T(8,128)} %get-tuple-element.251) | copy-start | bytes 9437188 | tf_op jit(solution)/shard_map/while
  221.2 3.3 %copy-start.1 = (f32[2,1024,384]{2,1,0:T(8,128)S(1)}, f32[2,1024,384]{2,1,0:T(8,128)}, u32[]{:S(2)}) copy-start(f32[2,1024,384]{2,1,0:T(8,128)} %get-tuple-element.251) | copy-start | bytes 9437188 | tf_op jit(solution)/shard_map/while
  229.0 3.3 %copy-start.1 = (f32[2,1024,384]{2,1,0:T(8,128)S(1)}, f32[2,1024,384]{2,1,0:T(8,128)}, u32[]{:S(2)}) copy-start(f32[2,1024,384]{2,1,0:T(8,128)} %get-tuple-element.251) | copy-start | bytes 9437188 | tf_op jit(solution)/shard_map/while
  256.8 9.8 %copy-start.4 = (f32[128,2]{0,1:T(2,128)S(1)}, f32[128,2]{0,1:T(2,128)}, u32[]{:S(2)}) copy-start(f32[128,2]{0,1:T(2,128)} %param.24) | copy-start | bytes 3076
  256.8 49.4 %copy-start.2 = (bf16[2048,256]{1,0:T(8,128)(2,1)S(1)}, bf16[2048,256]{1,0:T(8,128)(2,1)}, u32[]{:S(2)}) copy-start(bf16[2048,256]{1,0:T(8,128)(2,1)} %param.20) | copy-start | bytes 3145732
  260.7 27.0 %all-to-all-start.1 = ((bf16[32,1,16,256]{3,2,1,0:T(8,128)(2,1)}), bf16[32,1,16,256]{3,2,1,0:T(8,128)(2,1)S(1)}, u32[]{:S(2)}, u32[]{:S(2)}) async-start(bf16[32,1,16,256]{3,2,1,0:T(8,128)(2,1)} %fusion.48), calls=%async_computation.1 | async-start | bytes 524288 | tf_op jit(solution)/shard_map/all_to_all | solution.py:160
  (7 other events, 20.9 us)
Sparse Core Ops, SparseCore 0:
  10.6 88.9 all-gather.3
  156.0 51.7 all-gather.7
  257.8 48.3 all-gather.5
